TPU v7x, 256 devices: a whole 4x4x8 slice. The times are simulated.
256 devices in a mesh: kv: 64 (over z, x, core), tp: 4 (over y).
Axes of the slice: x: 4, y: 4, z: 8, core: 2. Of those that a mesh axis runs over, the one named last changes fastest.
Arguments:
- normed_input: bfloat16 [32768, 4096], P('kv', 'tp'), may hold values from -0.13183594 to 0.13183594
- queries: bfloat16 [32768, 2048], P('kv', 'tp'), may hold values from -1.5 to 1.5
- key_rows: bfloat16 [32768, 2048], P('kv', 'tp'), may hold values from -1.5 to 1.5
- value_rows: bfloat16 [32768, 2048], P('kv', 'tp'), may hold values from -6 to 6
- log_sums: float32 [32, 32768], P('tp', 'kv'), may hold values from -0.5 to 10
- cotangent: bfloat16 [32768, 2048], P('kv', 'tp'), may hold values from -48 to 48
- block_list: int32 [64, 16], P('kv'), may hold values from -1 to 1023, as said below
Outputs:
- grad_queries: float32 [32768, 2048], P('kv', 'tp')
- grad_keys: float32 [32768, 2048], P('kv', 'tp')
- grad_values: float32 [32768, 2048], P('kv', 'tp')
- grad_weight: float32 [4096, 2048], P('kv', 'tp')
Inputs may be any that keep to these rules, and one draw needn't show every extreme that they name: `block_list`: row d names the key blocks chosen by query block d: distinct blocks that all lie on devices of kv index below d (block g on index g // 16), at most 1 of them on one index, named entries first and -1 after them; row d has between min(8, d) and min(16, d) named entries, and the last row has 16 and names a block on index 0.
All inputs are finite; a program needn't handle non-finite values.
Results may differ from a plain program's by a relative error of at most 0.0041.
Values may be sent and summed in bfloat16 or wider, within the bound.
A program may use at most 128 MiB of HBM per device.

v0:
```python
import jax
import jax.numpy as jnp
from jax import lax
from jax.sharding import PartitionSpec as P

HD = 64
KB = 32
MOST = 16


def in_one_piece(arrays, axis, split_dim, concat_dim, along):
    both = jnp.concatenate(arrays, axis=along)
    filled, at, done = (
        lax.all_to_all(both, axis, split_axis=split_dim, concat_axis=concat_dim, tiled=True),
        0,
        [],
    )
    for a in arrays:
        done.append(lax.slice_in_dim(filled, at, at + a.shape[along], axis=along))
        at += a.shape[along]
    return tuple(done)


def contract(former, latter, former_dim, latter_dim):
    return lax.dot_general(
        former,
        latter,
        (((former_dim,), (latter_dim,)), ((), ())),
        preferred_element_type=jnp.float32,
    )


def head_terms(
    query_part, keys_own, values_own, keys_sel, values_sel, grad_out, log_sum, own_mask, sel_mask
):
    scaling = HD ** (-0.5)

    def forward(key_part, value_part, mask_part):
        scores = contract(query_part, key_part, 1, 1) * scaling
        probability = jnp.where(mask_part, jnp.exp(scores - log_sum[:, None]), 0.0)
        pulled = contract(grad_out, value_part, 1, 1)
        return (probability, pulled)

    prob_own, pull_own = forward(keys_own, values_own, own_mask)
    prob_sel, pull_sel = forward(keys_sel, values_sel, sel_mask)
    row_dot = jnp.sum(prob_own * pull_own, axis=1) + jnp.sum(prob_sel * pull_sel, axis=1)

    def backward(prob_part, pull_part, key_part):
        dscore = (prob_part * (pull_part - row_dot[:, None])).astype(jnp.bfloat16)
        rounded = prob_part.astype(jnp.bfloat16)
        return (
            contract(dscore, key_part, 1, 0),
            scaling * contract(dscore, query_part, 0, 0),
            contract(rounded, grad_out, 0, 0),
        )

    own_terms = backward(prob_own, pull_own, keys_own)
    sel_terms = backward(prob_sel, pull_sel, keys_sel)
    return (
        scaling * (own_terms[0] + sel_terms[0]),
        own_terms[1],
        own_terms[2],
        sel_terms[1],
        sel_terms[2],
    )


def heads_first(array):
    return array.reshape(array.shape[0], -1, HD).transpose(1, 0, 2)


def tokens_first(array):
    return array.transpose(1, 0, 2).reshape(array.shape[1], -1)


def per_device(normed_input, queries, key_rows, value_rows, log_sums, cotangent, block_list):
    rows_here, width_here = queries.shape
    kv_size = lax.axis_size("kv")
    capacity = max(1, 2 * MOST // kv_size)
    slot_count = kv_size * capacity
    block_count = rows_here // KB
    chosen = block_list[0]
    listed = chosen >= 0
    owner_dev = jnp.where(listed, chosen // block_count, kv_size)
    owner_block = jnp.where(listed, chosen % block_count, 0)
    turn_order = jnp.arange(MOST)
    earlier = (owner_dev[:, None] == owner_dev[None, :]) & (
        turn_order[None, :] < turn_order[:, None]
    )
    ranked = jnp.sum(earlier.astype(jnp.int32), axis=1)
    slot_of = jnp.where(listed, owner_dev * capacity + ranked, slot_count)
    matched = slot_of[:, None] == jnp.arange(slot_count)[None, :]
    wanted = jnp.max(jnp.where(matched, owner_block[:, None], -1), axis=0)
    requested = lax.all_to_all(
        wanted.reshape(kv_size, capacity), "kv", split_axis=0, concat_axis=0, tiled=True
    ).reshape(slot_count)
    clipped = jnp.clip(requested, 0, block_count - 1)
    send_keys = key_rows.reshape(block_count, KB, width_here)[clipped]
    send_values = value_rows.reshape(block_count, KB, width_here)[clipped]
    got_keys, got_values = in_one_piece((send_keys, send_values), "kv", 0, 0, 1)
    picked = jnp.where(listed, slot_of, 0)
    keys_sel = got_keys[picked].reshape(MOST * KB, width_here)
    values_sel = got_values[picked].reshape(MOST * KB, width_here)
    live_keys = jnp.repeat(listed, KB)
    position = jnp.arange(rows_here)
    own_mask = position[:, None] >= position[None, :]
    sel_mask = jnp.broadcast_to(live_keys[None, :], (rows_here, live_keys.shape[0]))

    def per_head(pieces):
        query_part, keys_own, values_own, key_part, value_part, grad_out, log_sum = pieces
        return head_terms(
            query_part,
            keys_own,
            values_own,
            key_part,
            value_part,
            grad_out,
            log_sum,
            own_mask,
            sel_mask,
        )

    results = lax.map(
        per_head,
        (
            heads_first(queries),
            heads_first(key_rows),
            heads_first(value_rows),
            heads_first(keys_sel),
            heads_first(values_sel),
            heads_first(cotangent),
            log_sums,
        ),
    )
    grad_queries = tokens_first(results[0])
    sel_key_grad = tokens_first(results[3]).astype(jnp.bfloat16)
    sel_value_grad = tokens_first(results[4]).astype(jnp.bfloat16)
    target = jnp.where(listed, slot_of, slot_count)
    back_keys = (
        jnp.zeros((slot_count, KB, width_here), jnp.bfloat16)
        .at[target]
        .set(sel_key_grad.reshape(MOST, KB, width_here), mode="drop")
    )
    back_values = (
        jnp.zeros((slot_count, KB, width_here), jnp.bfloat16)
        .at[target]
        .set(sel_value_grad.reshape(MOST, KB, width_here), mode="drop")
    )
    returned_keys, returned_values = in_one_piece((back_keys, back_values), "kv", 0, 0, 1)
    slot_keys = returned_keys.reshape(slot_count, KB * width_here).astype(jnp.float32)
    slot_values = returned_values.reshape(slot_count, KB * width_here).astype(jnp.float32)
    indicator = (requested[None, :] == jnp.arange(block_count)[:, None]).astype(jnp.float32)
    added_keys = jnp.dot(indicator, slot_keys, precision=lax.Precision.HIGHEST)
    added_values = jnp.dot(indicator, slot_values, precision=lax.Precision.HIGHEST)
    grad_keys = tokens_first(results[1]) + added_keys.reshape(rows_here, width_here)
    grad_values = tokens_first(results[2]) + added_values.reshape(rows_here, width_here)
    rounded = grad_queries.astype(jnp.bfloat16)
    gathered = lax.all_gather(normed_input, "tp", axis=1, tiled=True)
    grad_weight = lax.psum_scatter(
        contract(gathered, rounded, 0, 0), "kv", scatter_dimension=0, tiled=True
    )
    return (grad_queries, grad_keys, grad_values, grad_weight)


def solution(mesh):
    return jax.shard_map(
        per_device,
        mesh=mesh,
        in_specs=(
            P("kv", "tp"),
            P("kv", "tp"),
            P("kv", "tp"),
            P("kv", "tp"),
            P("tp", "kv"),
            P("kv", "tp"),
            P("kv", None),
        ),
        out_specs=(P("kv", "tp"), P("kv", "tp"), P("kv", "tp"), P("kv", "tp")),
        check_vma=False,
    )
```

profile of v0, /device:TPU:73, one launch (start us, length us, event | category | flops | bytes accessed | tf_op | source)
XLA Modules:
  0.0 435.3 jit_solution(7500977006591494147)
XLA Ops:
  9.5 18.7 %all_to_all.19 = s32[64,1,1]{2,1,0:T(1,128)S(1)} all-to-all(s32[64,1,1]{2,1,0:T(1,128)S(1)} %copy.75), channel_id=1, replica_groups=mesh['kv'=64,'tp'=4] {'kv'}, dimensions={0} | all-to-all | bytes 512 | tf_op jit(solution)/shard_map/all_to_all | solution.py:94
  28.3 2.4 fusion.74
  30.7 1.8 gather_fusion.1
  32.5 2.0 gather_fusion
  34.5 3.9 pad_maximum_fusion
  38.4 7.7 %all-to-all-start.1 = ((bf16[64,64,512]{2,1,0:T(8,128)(2,1)}), bf16[64,64,512]{2,1,0:T(8,128)(2,1)}, u32[]{:S(2)}, u32[]{:S(2)}) async-start(bf16[64,64,512]{2,1,0:T(8,128)(2,1)} %pad_maximum_fusion), calls=%async_computation.1 | async-start | bytes 8388608 | tf_op jit(solution)/shard_map/all_to_all | solution.py:14
  49.9 89.1 %all-to-all-done.1 = bf16[64,64,512]{2,1,0:T(8,128)(2,1)} async-done(((bf16[64,64,512]{2,1,0:T(8,128)(2,1)}), bf16[64,64,512]{2,1,0:T(8,128)(2,1)}, u32[]{:S(2)}, u32[]{:S(2)}) %all-to-all-start.1) | async-done | bytes 4194336 | tf_op jit(solution)/shard_map/all_to_all | solution.py:14
  139.0 4.0 fusion.76
  143.1 3.0 gather_fusion.3
  152.0 88.0 %while.19 = (s32[]{:T(128)}, f32[8,512,64]{1,2,0:T(8,128)}, f32[8,512,64]{1,2,0:T(8,128)}, f32[8,512,64]{1,2,0:T(8,128)}, bf16[8,512,64]{1,2,0:T(8,128)(2,1)}, /...) while((s32[]{:T(128)}, f32[8,512,64]{1,2,0:T(8,128)}, ...), condition=%wide.region_5.6_spmd.clone, body=%wide.region_2.5_spmd.clone.sunk | while | flops 340655616 | bytes 17790620 | solution.py:123
  171.3 1.7 fusion.127
  204.3 1.7 fusion.127
  226.4 1.7 fusion.127
  237.4 1.7 fusion.127
  240.0 8.1 %convolution_bitcast_fusion.2 = f32[4096,512]{0,1:T(8,128)} fusion(bf16[512,4096]{1,0:T(8,128)(2,1)} %all-gather.2.cloned.1.call-done, f32[512,512]{0,1:T(8,128)} %bitcast.239), kind=kOutput, calls=%fused_computation.79 | convolution fusion | flops 2147745792 | bytes 13631488 | tf_op jit(solution)/shard_map/dot_general | solution.py:25
  248.1 9.0 %copy.90 = f32[4096,512]{1,0:T(8,128)} copy(f32[4096,512]{0,1:T(8,128)} %convolution_bitcast_fusion.2) | data formatting | bytes 16777216
  262.6 2.6 scatter_fusion.1
  266.5 4.0 pad_maximum_fusion.1
  270.5 9.1 %all-to-all-start.2 = ((bf16[64,64,512]{2,1,0:T(8,128)(2,1)}), bf16[64,64,512]{2,1,0:T(8,128)(2,1)}, u32[]{:S(2)}, u32[]{:S(2)}) async-start(bf16[64,64,512]{2,1,0:T(8,128)(2,1)} %pad_maximum_fusion.1), calls=%async_computation.2 | async-start | bytes 8388608 | tf_op jit(solution)/shard_map/all_to_all | solution.py:14
  280.9 104.7 %all-to-all-done.2 = bf16[64,64,512]{2,1,0:T(8,128)(2,1)} async-done(((bf16[64,64,512]{2,1,0:T(8,128)(2,1)}), bf16[64,64,512]{2,1,0:T(8,128)(2,1)}, u32[]{:S(2)}, u32[]{:S(2)}) %all-to-all-start.2) | async-done | bytes 4194336 | tf_op jit(solution)/shard_map/all_to_all | solution.py:14
  385.6 2.6 fusion.75
  394.8 3.1 bitcast_add_fusion
  397.9 2.5 copy.88
  401.7 26.7 %reduce-scatter.4.cloned.1.call-done = f32[64,512]{1,0:T(8,128)} async-done(((f32[4096,512]{1,0:T(8,128)}), f32[64,512]{1,0:T(8,128)}) %reduce-scatter.4.cloned.1.call-update) | async-done | bytes 131088
  (166 shorter events, 108.8 us)
Async XLA Ops:
  30.7 1.8 copy-start
  38.4 100.6 %all-to-all-start.1 = ((bf16[64,64,512]{2,1,0:T(8,128)(2,1)}), bf16[64,64,512]{2,1,0:T(8,128)(2,1)}, u32[]{:S(2)}, u32[]{:S(2)}) async-start(bf16[64,64,512]{2,1,0:T(8,128)(2,1)} %pad_maximum_fusion), calls=%async_computation.1 | async-start | bytes 8388608 | tf_op jit(solution)/shard_map/all_to_all | solution.py:14
  46.1 2.0 copy-start.1
  46.1 3.1 copy-start.7
  46.1 3.2 copy-start.5
  46.1 3.5 copy-start.6
  46.2 193.8 %all-gather.2.cloned.1.call-start = ((), (), s32[]{:S(2)}) async-start(), calls=%async_computation.4 | async-start | bytes 5242880 | tf_op jit(solution)/shard_map/all_gather | solution.py:158
  46.9 381.5 %reduce-scatter.4.cloned.1.call-start = ((), (), s32[]{:S(2)}) async-start(), calls=%async_computation.5 | async-start | bytes 8519680
  257.1 1.0 copy-start.3
  257.1 2.4 copy-start.4
  270.5 9.1 %copy-start.2 = (f32[8,512,64]{1,2,0:T(8,128)S(1)}, f32[8,512,64]{1,2,0:T(8,128)}, u32[]{:S(2)}) copy-start(f32[8,512,64]{1,2,0:T(8,128)} %get-tuple-element.85) | copy-start | bytes 3145732
  270.5 115.1 %all-to-all-start.2 = ((bf16[64,64,512]{2,1,0:T(8,128)(2,1)}), bf16[64,64,512]{2,1,0:T(8,128)(2,1)}, u32[]{:S(2)}, u32[]{:S(2)}) async-start(bf16[64,64,512]{2,1,0:T(8,128)(2,1)} %pad_maximum_fusion.1), calls=%async_computation.2 | async-start | bytes 8388608 | tf_op jit(solution)/shard_map/all_to_all | solution.py:14
Sparse Core Ops, SparseCore 0:
  48.8 50.9 all-gather.1
  257.3 171.1 reduce-scatter.3
where the time goes:
time: 444 us; the launch traced here: 435 us
  waiting for transfers between devices  221 us (50%)
  matrix products  86.3 us (19%)
  local copies, waits for them, and re-layouts  57.1 us (13%)
  other arithmetic  20.2 us (5%)
  blocking collectives  18.7 us (4%)
  starting transfers between devices  17 us (4%)
  between operations  14.3 us (3%)
    all_to_all x2, waiting for transfers between devices, in_one_piece(): lax.all_to_all(both, axis, split_axis=split_dim, concat_axis=concat_dim,...  194 us
    dot_general x81, matrix products, contract(): lax.dot_general(former, latter, (((former_dim,), (latter_dim,)), ((), ())...  85.5 us
    unnamed x3, waiting for transfers between devices  27.4 us
    unnamed x28, local copies, waits for them, and re-layouts  21.5 us
    all_to_all x1, blocking collectives, per_device(): lax.all_to_all(wanted.reshape(kv_size, capacity), 'kv', split_axis=0, con...  18.7 us
    all_to_all x2, starting transfers between devices, in_one_piece(): lax.all_to_all(both, axis, split_axis=split_dim, concat_axis=concat_dim,...  16.8 us
  transfers between devices with their start and end apart: 4, of which 3 were waited for; matrix products, arithmetic and copies ran while one was open for 31% of the time, Pallas kernels for 0%

commit v1 on v0

v1 whole, which is shorter than its diff:
```python
import functools

import jax
import jax.numpy as jnp
from jax import lax
from jax.experimental import pallas as pl
from jax.experimental.pallas import tpu as pltpu
from jax.sharding import PartitionSpec as P

MESH = pl.DeviceIdType.MESH
HD = 64
KB = 32
MOST = 16
TOK = 512
NZ = 8
NG = 8
NY = 4
NX = 4
SLOTS = NZ * (NZ + 1) // 2
BPD = TOK // KB
F32 = jnp.float32
BF16 = jnp.bfloat16
Z_ORDER = (4, 3, 5, 2, 6, 1, 7)
G_ORDER = (4, 5, 3, 2, 6, 7, 1)


def here():
    kv = lax.axis_index("kv")
    return kv, lax.div(kv, NG), lax.rem(kv, NG), lax.axis_index("tp")


def remote(src, dst, send_sem, recv_sem, target):
    return pltpu.make_async_remote_copy(
        src_ref=src, dst_ref=dst, send_sem=send_sem, recv_sem=recv_sem, device_id=target, device_id_type=MESH
    )


def signal(sem, target):
    pl.semaphore_signal(sem, inc=1, device_id=target, device_id_type=MESH)


def gather_kernel(
    q_ref, k_ref, v_ref, o_ref, lse_ref, list_ref, a_ref,
    kvr_ref, qor_ref, lser_ref, xr_ref, ag_ref, t_ref, w_ref,
    kvp, qop, lsp, tb, xs, wsm,
    kv_s, kv_r, qo_s, qo_r, ls_s, ls_r, tb_s, tb_r, xs_s, xs_r, a_s, a_r, loc,
):
    kv, z, g, y = here()
    right, left = lax.rem(y + 1, NY), lax.rem(y + NY - 1, NY)
    planes = NZ * NG

    bar = pltpu.get_barrier_semaphore()

    def greet(i, c):
        signal(bar, {"kv": lax.rem(kv + i, planes)})
        return c

    lax.fori_loop(1, planes, greet, 0)
    signal(bar, {"tp": right})
    signal(bar, {"tp": left})

    rows = 64
    low = lax.broadcasted_iota(jnp.int32, (rows, 128), 1) < HD

    def pack(i, c):
        r = pl.ds(pl.multiple_of(i * rows, rows), rows)
        for first, second, out in ((k_ref, v_ref, kvp), (q_ref, o_ref, qop)):
            for p in range(4):
                a = first[r, 128 * p : 128 * p + 128].astype(F32)
                b = second[r, 128 * p : 128 * p + 128].astype(F32)
                first_head = jnp.where(low, a, pltpu.roll(b, HD, 1)).astype(BF16)
                second_head = jnp.where(low, pltpu.roll(a, HD, 1), b).astype(BF16)
                for j in range(rows // KB):
                    at = i * (rows // KB) + j
                    out[2 * p, at] = first_head[KB * j : KB * j + KB]
                    out[2 * p + 1, at] = second_head[KB * j : KB * j + KB]
        return c

    lax.fori_loop(0, TOK // rows, pack, 0)
    for h in range(NZ):
        lsp[h] = lse_ref[h : h + 1, :]
    tb[kv] = list_ref[...]
    kvr_ref[z] = kvp[z]

    pl.semaphore_wait(bar, planes - 1 + 2)

    def table_copy(peer, slot):
        return remote(tb.at[slot], tb.at[slot], tb_s.at[peer], tb_r.at[slot], {"kv": peer})

    def send_table(i, c):
        table_copy(lax.rem(kv + i, planes), kv).start()
        return c

    lax.fori_loop(1, planes, send_table, 0)

    to_right = remote(a_ref, ag_ref.at[0], a_s.at[0], a_r.at[0], {"tp": right})
    to_left = remote(a_ref, ag_ref.at[1], a_s.at[1], a_r.at[1], {"tp": left})
    to_right.start()
    to_left.start()

    def kv_copy(zt, slot):
        return remote(kvp.at[zt], kvr_ref.at[slot], kv_s.at[zt], kv_r.at[slot], {"kv": zt * NG + g})

    def qo_copy(zt, slot):
        return remote(qop.at[zt], qor_ref.at[slot], qo_s.at[zt], qo_r.at[slot], {"kv": zt * NG + g})

    def ls_copy(zt, slot):
        return remote(lsp.at[zt], lser_ref.at[slot], ls_s.at[zt], ls_r.at[slot], {"kv": zt * NG + g})

    for off in Z_ORDER:
        kv_copy(lax.rem(z + off, NZ), z).start()
    for off in Z_ORDER:
        zt = lax.rem(z + off, NZ)
        qo_copy(zt, z).start()
        ls_copy(zt, z).start()
    own_qo = pltpu.make_async_copy(qop.at[z], qor_ref.at[z], loc.at[0])
    own_ls = pltpu.make_async_copy(lsp.at[z], lser_ref.at[z], loc.at[1])
    own_qo.start()
    own_ls.start()

    def wait_table(i, c):
        peer = lax.rem(kv + i, planes)
        table_copy(peer, peer).wait_recv()
        return c

    lax.fori_loop(1, planes, wait_table, 0)

    table = tb[:, 0, :]
    t_ref[...] = table
    lanes = lax.broadcasted_iota(jnp.int32, (planes, 128), 1)
    want = jnp.full((planes, 128), -1, jnp.int32)
    for s in range(MOST):
        col = table[:, s : s + 1]
        want = jnp.where(lax.shift_right_arithmetic(col, 4) == lanes, jnp.bitwise_and(col, BPD - 1), want)
    w_ref[...] = want
    to_smem = pltpu.make_async_copy(w_ref, wsm, loc.at[2])
    to_smem.start()
    to_smem.wait()

    for off in Z_ORDER:
        zs = lax.rem(z + NZ - off, NZ)
        kv_copy(zs, zs).wait_recv()

    def x_copy(gp, slot):
        return remote(xs.at[gp], xr_ref.at[slot], xs_s.at[gp], xs_r.at[slot], {"kv": z * NG + gp})

    def choose(gp):
        for zd in range(NZ):
            for zo in range(zd + 1):
                b = jnp.maximum(wsm[zd * NG + gp, zo * NG + g], 0)
                xs[gp, zd * (zd + 1) // 2 + zo] = kvr_ref[zo, b]

    def pick(i, c):
        gp = lax.rem(g + i, NG)
        choose(gp)
        x_copy(gp, g).start()
        return c

    lax.fori_loop(1, NG, pick, 0)
    choose(g)
    own_x = pltpu.make_async_copy(xs.at[g], xr_ref.at[g], loc.at[3])
    own_x.start()

    half = TOK // 2
    on_right = remote(
        ag_ref.at[0, pl.ds(0, half)], ag_ref.at[2, pl.ds(0, half)], a_s.at[2], a_r.at[2], {"tp": right}
    )
    on_left = remote(
        ag_ref.at[1, pl.ds(half, half)], ag_ref.at[2, pl.ds(half, half)], a_s.at[3], a_r.at[3], {"tp": left}
    )
    to_right.wait_recv()
    on_right.start()
    to_left.wait_recv()
    on_left.start()

    for off in Z_ORDER:
        zs = lax.rem(z + NZ - off, NZ)
        qo_copy(zs, zs).wait_recv()
        ls_copy(zs, zs).wait_recv()

    def wait_x(i, c):
        gp = lax.rem(g + i, NG)
        x_copy(gp, gp).wait_recv()
        x_copy(gp, g).wait_send()
        return c

    lax.fori_loop(1, NG, wait_x, 0)

    def drain_table(i, c):
        table_copy(lax.rem(kv + i, planes), kv).wait_send()
        return c

    lax.fori_loop(1, planes, drain_table, 0)
    for off in Z_ORDER:
        zt = lax.rem(z + off, NZ)
        kv_copy(zt, z).wait_send()
        qo_copy(zt, z).wait_send()
        ls_copy(zt, z).wait_send()
    to_right.wait_send()
    to_left.wait_send()
    on_right.wait()
    on_left.wait()
    own_qo.wait()
    own_ls.wait()
    own_x.wait()


def attention_kernel(t_ref, qo_ref, kv_ref, lse_ref, xr_ref, dq_ref, dkvo_ref, rb_ref, sel, qs, om, p_scr, u_scr, rd, dq):
    zd = pl.program_id(0)
    g = lax.rem(lax.axis_index("kv"), NG)
    d = zd * NG + g
    base = lax.div(zd * (zd + 1), 2)

    @pl.when(zd == 0)
    def _():
        rb_ref[...] = jnp.zeros_like(rb_ref)

    count = jnp.int32(0)
    for s in range(MOST):
        entry = t_ref[d, s]
        count = count + jnp.where(entry >= 0, 1, 0)
        owner = lax.shift_right_arithmetic(jnp.maximum(entry, 0), 4)
        sel[KB * s : KB * s + KB, :] = xr_ref[jnp.bitwise_and(owner, NG - 1), base + lax.shift_right_arithmetic(owner, 3)]

    low = lax.broadcasted_iota(jnp.int32, (TOK, 128), 1) < HD
    both = qo_ref[0].reshape(TOK, 128).astype(F32)
    qs[...] = jnp.where(low, both * (HD ** -0.5), 0.0).astype(BF16)
    om[...] = jnp.where(low, 0.0, both).astype(BF16)
    rd[...] = jnp.zeros_like(rd)
    dq[...] = jnp.zeros_like(dq)
    half = TOK // 2
    nt = (((1,), (1,)), ((), ()))

    def forward(block, row, q0):
        st = lax.dot_general(block, qs[q0:, :], nt, preferred_element_type=F32)
        ut = lax.dot_general(block, om[q0:, :], nt, preferred_element_type=F32)
        key = lax.broadcasted_iota(jnp.int32, st.shape, 0) + (row % TOK)
        if row < TOK:
            keep = key <= lax.broadcasted_iota(jnp.int32, st.shape, 1) + q0
        else:
            keep = key < count * KB
        p = jnp.where(keep, jnp.exp(st - lse_ref[0, :, q0:]), 0.0)
        p_scr[row : row + half, q0:] = p
        u_scr[row : row + half, q0:] = ut
        rd[:, q0:] += jnp.sum(p * ut, axis=0, keepdims=True)

    def backward(block, row, q0):
        p = p_scr[row : row + half, q0:]
        ds = (p * (u_scr[row : row + half, q0:] - rd[:, q0:])).astype(BF16)
        dq[:, q0:] += jnp.dot(block.T[:HD, :], ds, preferred_element_type=F32)
        dkv = jnp.dot(ds, qs[q0:, :], preferred_element_type=F32)
        dkv += jnp.dot(p.astype(BF16), om[q0:, :], preferred_element_type=F32)
        if row < TOK:
            dkvo_ref[0, row : row + half, :] = dkv
            return
        dkv = dkv.astype(BF16)
        for i in range(half // KB):
            entry = t_ref[d, (row - TOK) // KB + i]
            owner = lax.shift_right_arithmetic(entry, 4)

            @pl.when(entry >= 0)
            def _(i=i, owner=owner):
                rb_ref[jnp.bitwise_and(owner, NG - 1), base + lax.shift_right_arithmetic(owner, 3)] = dkv[
                    KB * i : KB * i + KB
                ]

    own = kv_ref[0].reshape(TOK, 128)
    forward(own[:half], 0, 0)
    forward(own[half:], half, half)
    forward(sel[:half, :], TOK, 0)
    pl.when(count > MOST // 2)(lambda: forward(sel[half:, :], TOK + half, 0))
    backward(own[:half], 0, 0)
    backward(own[half:], half, half)
    backward(sel[:half, :], TOK, 0)
    pl.when(count > MOST // 2)(lambda: backward(sel[half:, :], TOK + half, 0))
    dq_ref[0] = (dq[...] * (HD ** -0.5)).astype(BF16)


def product_kernel(
    dq_ref, rb_ref, a_ref, ag_ref,
    qbt_ref, rbr_ref, s1_ref,
    abuf, qb, keep, cs, cr,
    dq_s, dq_r, rb_s, rb_r, c_s, c_r, loc,
):
    kv, z, g, y = here()
    core = lax.rem(kv, 2)
    partner = kv + 1 - 2 * core
    loads = [pltpu.make_async_copy(a_ref, abuf.at[0], loc.at[0])]
    loads += [pltpu.make_async_copy(ag_ref.at[j], abuf.at[j + 1], loc.at[j + 1]) for j in range(NY - 1)]
    bar = pltpu.get_barrier_semaphore()
    for i in range(1, NZ):
        signal(bar, {"kv": lax.rem(z + i, NZ) * NG + g})
        signal(bar, {"kv": z * NG + lax.rem(g + i, NG)})
    for load in loads:
        load.start()
    qbt_ref[z] = dq_ref[z]
    pl.semaphore_wait(bar, NZ - 1 + NG - 1)

    def dq_copy(zt, slot):
        return remote(dq_ref.at[zt], qbt_ref.at[slot], dq_s.at[zt], dq_r.at[slot], {"kv": zt * NG + g})

    def rb_copy(gp, slot):
        return remote(rb_ref.at[gp], rbr_ref.at[slot], rb_s.at[gp], rb_r.at[slot], {"kv": z * NG + gp})

    for off in Z_ORDER:
        dq_copy(lax.rem(z + off, NZ), z).start()
    for off in G_ORDER:
        rb_copy(lax.rem(g + off, NG), g).start()
    own_rb = pltpu.make_async_copy(rb_ref.at[g], rbr_ref.at[g], loc.at[NY])
    own_rb.start()
    for off in Z_ORDER:
        zs = lax.rem(z + NZ - off, NZ)
        dq_copy(zs, zs).wait_recv()

    for h in range(NZ):
        qb[:, HD * h : HD * h + HD] = qbt_ref[h].astype(F32).T.astype(BF16)

    def core_copy(yb):
        part = pl.ds(yb * 8, 8)
        return remote(cs.at[part], cr.at[part], c_s.at[yb], c_r.at[yb], {"kv": partner})

    owners = (y, lax.rem(y + NY - 1, NY), lax.rem(y + 1, NY), lax.rem(y + 2, NY))
    for j in range(NY):
        loads[j].wait()
        yb = owners[j]

        def strip(m, c, j=j, yb=yb):
            a = abuf[j, :, pl.ds(pl.multiple_of(m * 128, 128), 128)]
            acc = lax.dot_general(a, qb[...], (((0,), (0,)), ((), ())), preferred_element_type=F32)
            lo, hi = acc[:HD, :], acc[HD:, :]
            keep[yb * 8 + m] = jnp.where(core == 0, lo, hi)
            cs[yb * 8 + m] = jnp.where(core == 0, hi, lo).astype(BF16)
            return c

        lax.fori_loop(0, 8, strip, 0)
        core_copy(yb).start()
    for j in range(NY):
        yb = owners[j]
        core_copy(yb).wait_recv()

        def add(m, c, yb=yb):
            i = yb * 8 + m
            s1_ref[i] = (keep[i] + cr[i].astype(F32)).astype(BF16)
            return c

        lax.fori_loop(0, 8, add, 0)

    for off in G_ORDER:
        gp = lax.rem(g + off, NG)
        rb_copy(gp, gp).wait_recv()
        rb_copy(gp, g).wait_send()
    for off in Z_ORDER:
        dq_copy(lax.rem(z + off, NZ), z).wait_send()
    for j in range(NY):
        core_copy(owners[j]).wait_send()
    own_rb.wait()


def collect_kernel(w_ref, own_ref, rbr_ref, out_ref, acc):
    zo = pl.program_id(0)
    o = zo * NG + lax.rem(lax.axis_index("kv"), NG)
    acc[...] = own_ref[0]

    def add(zd, c):
        for gd in range(NG):
            b = w_ref[zd * NG + gd, o]

            @pl.when(b >= 0)
            def _(b=b, gd=gd):
                at = pl.ds(pl.multiple_of(b * KB, KB), KB)
                acc[at, :] += rbr_ref[gd, lax.div(zd * (zd + 1), 2) + zo].astype(F32)

        return c

    lax.fori_loop(zo, NZ, add, 0)
    out_ref[0] = acc[...].astype(BF16)


def return_kernel(
    dkv_ref, s1_ref,
    dkvr_ref, gw_ref,
    relay, fixed, last_l, last_r, s2, zr,
    dk_s, dk_r, f_s, f_r, n_s, n_r, l_s, l_r, z_s, z_r, loc,
):
    kv, z, g, y = here()
    core = lax.rem(kv, 2)
    x = lax.div(g, 2)

    def at_x(t):
        return {"kv": z * NG + lax.rem(t, NX) * 2 + core}

    right, left, far = x + 1, x + NX - 1, lax.rem(x + 2, NX)
    bar = pltpu.get_barrier_semaphore()
    for i in range(1, NZ):
        signal(bar, {"kv": lax.rem(z + i, NZ) * NG + g})
    signal(bar, at_x(right))
    signal(bar, at_x(left))
    pl.semaphore_wait(bar, NZ - 1 + 2)

    def piece(zz, t):
        return zz * NX + lax.rem(t, NX)

    def first(zz):
        ahead = right if zz % 2 == 0 else left
        return remote(s1_ref.at[piece(zz, far)], relay.at[zz], f_s.at[zz], f_r.at[zz], at_x(ahead))

    def direct(zz):
        back = left if zz % 2 == 0 else right
        into = last_r if zz % 2 == 0 else last_l
        return remote(s1_ref.at[piece(zz, back)], into.at[zz], n_s.at[zz], n_r.at[zz], at_x(back))

    def summed(zz):
        ahead = right if zz % 2 == 0 else left
        into = last_l if zz % 2 == 0 else last_r
        return remote(fixed.at[zz], into.at[zz], l_s.at[zz], l_r.at[zz], at_x(ahead))

    def dkv_copy(zt, slot):
        return remote(dkv_ref.at[zt], dkvr_ref.at[slot], dk_s.at[zt], dk_r.at[slot], {"kv": zt * NG + g})

    for zz in range(NZ):
        first(zz).start()
    for zz in range(NZ):
        direct(zz).start()
    for off in Z_ORDER:
        dkv_copy(lax.rem(z + off, NZ), z).start()
    own = pltpu.make_async_copy(dkv_ref.at[z], dkvr_ref.at[z], loc.at[0])
    own.start()

    for zz in range(NZ):
        ahead = right if zz % 2 == 0 else left
        first(zz).wait_recv()
        fixed[zz] = (relay[zz].astype(F32) + s1_ref[piece(zz, ahead)].astype(F32)).astype(BF16)
        summed(zz).start()

    def z_copy(zt, slot):
        return remote(s2.at[zt], zr.at[slot], z_s.at[zt], z_r.at[slot], {"kv": zt * NG + g})

    for zz in range(NZ):
        direct(zz).wait_recv()
        summed(zz).wait_recv()
        total = s1_ref[piece(zz, x)].astype(F32) + last_l[zz].astype(F32) + last_r[zz].astype(F32)
        s2[zz] = total.astype(BF16)

        @pl.when(zz != z)
        def _(zz=zz):
            z_copy(zz, z).start()

        @pl.when(zz == z)
        def _(total=total):
            gw_ref[...] = total

    for off in range(1, NZ):
        zs = lax.rem(z + off, NZ)
        z_copy(zs, zs).wait_recv()
        gw_ref[...] += zr[zs].astype(F32)

    for off in Z_ORDER:
        zs = lax.rem(z + NZ - off, NZ)
        dkv_copy(zs, zs).wait_recv()
    for zz in range(NZ):
        first(zz).wait_send()
        direct(zz).wait_send()
        summed(zz).wait_send()
    for off in Z_ORDER:
        zt = lax.rem(z + off, NZ)
        dkv_copy(zt, z).wait_send()
        z_copy(zt, z).wait_send()
    own.wait()


def unpack_kernel(qbt_ref, dkv_ref, gq_ref, gk_ref, gv_ref):
    gq_ref[...] = qbt_ref[...].astype(F32).reshape(128, TOK).T
    a = dkv_ref[0].astype(F32)
    b = dkv_ref[1].astype(F32)
    low = lax.broadcasted_iota(jnp.int32, (TOK, 128), 1) < HD
    gk_ref[...] = jnp.where(low, a, pltpu.roll(b, HD, 1))
    gv_ref[...] = jnp.where(low, pltpu.roll(a, HD, 1), b)


def per_device(normed_input, queries, key_rows, value_rows, log_sums, cotangent, block_list):
    vmem = pl.BlockSpec(memory_space=pltpu.VMEM)
    smem = pl.BlockSpec(memory_space=pltpu.SMEM)
    hbm = pl.BlockSpec(memory_space=pl.ANY)
    dma = pltpu.SemaphoreType.DMA
    shape = jax.ShapeDtypeStruct
    planes = NZ * NG
    listed = jnp.pad(block_list, ((0, 7), (0, 128 - MOST)), constant_values=-1)

    kvr, qor, lser, xr, ag, table, want = pl.pallas_call(
        gather_kernel,
        out_shape=(
            shape((NZ, BPD, KB, 128), BF16),
            shape((NZ, BPD, KB, 128), BF16),
            shape((NZ, 1, TOK), F32),
            shape((NG, SLOTS, KB, 128), BF16),
            shape((NY - 1, TOK, normed_input.shape[1]), BF16),
            shape((planes, 128), jnp.int32),
            shape((planes, 128), jnp.int32),
        ),
        in_specs=[vmem] * 6 + [hbm],
        out_specs=(vmem, hbm, hbm, hbm, hbm, vmem, vmem),
        scratch_shapes=[
            pltpu.VMEM((NZ, BPD, KB, 128), BF16),
            pltpu.VMEM((NZ, BPD, KB, 128), BF16),
            pltpu.VMEM((NZ, 1, TOK), F32),
            pltpu.VMEM((planes, 8, 128), jnp.int32),
            pltpu.VMEM((NG, SLOTS, KB, 128), BF16),
            pltpu.SMEM((planes, 128), jnp.int32),
            dma((NZ,)), dma((NZ,)), dma((NZ,)), dma((NZ,)), dma((NZ,)), dma((NZ,)),
            dma((planes,)), dma((planes,)), dma((NG,)), dma((NG,)), dma((4,)), dma((4,)), dma((4,)),
        ],
        compiler_params=pltpu.CompilerParams(collective_id=0, has_side_effects=True),
        name="gather",
    )(queries, key_rows, value_rows, cotangent, log_sums, listed, normed_input)

    dqt, dkvo, rb = pl.pallas_call(
        attention_kernel,
        grid=(NZ,),
        out_shape=(
            shape((NZ, HD, TOK), BF16),
            shape((NZ, TOK, 128), F32),
            shape((NG, SLOTS, KB, 128), BF16),
        ),
        in_specs=[
            smem,
            pl.BlockSpec((1, BPD, KB, 128), lambda i: (i, 0, 0, 0)),
            pl.BlockSpec((1, BPD, KB, 128), lambda i: (i, 0, 0, 0)),
            pl.BlockSpec((1, 1, TOK), lambda i: (i, 0, 0)),
            pl.BlockSpec((NG, SLOTS, KB, 128), lambda i: (0, 0, 0, 0)),
        ],
        out_specs=(
            pl.BlockSpec((1, HD, TOK), lambda i: (i, 0, 0)),
            pl.BlockSpec((1, TOK, 128), lambda i: (i, 0, 0)),
            pl.BlockSpec((NG, SLOTS, KB, 128), lambda i: (0, 0, 0, 0)),
        ),
        scratch_shapes=[
            pltpu.VMEM((TOK, 128), BF16),
            pltpu.VMEM((TOK, 128), BF16),
            pltpu.VMEM((TOK, 128), BF16),
            pltpu.VMEM((2 * TOK, TOK), F32),
            pltpu.VMEM((2 * TOK, TOK), F32),
            pltpu.VMEM((1, TOK), F32),
            pltpu.VMEM((HD, TOK), F32),
        ],
        compiler_params=pltpu.CompilerParams(dimension_semantics=("arbitrary",)),
        name="attention",
    )(table, qor, kvr, lser, xr)

    qbt, rbr, s1 = pl.pallas_call(
        product_kernel,
        out_shape=(
            shape((NZ, HD, TOK), BF16),
            shape((NG, SLOTS, KB, 128), BF16),
            shape((NZ * NX, HD, TOK), BF16),
        ),
        in_specs=[vmem, vmem, hbm, hbm],
        out_specs=(vmem, hbm, vmem),
        scratch_shapes=[
            pltpu.VMEM((NY, TOK, normed_input.shape[1]), BF16),
            pltpu.VMEM((TOK, NZ * HD), BF16),
            pltpu.VMEM((NZ * NX, HD, TOK), F32),
            pltpu.VMEM((NZ * NX, HD, TOK), BF16),
            pltpu.VMEM((NZ * NX, HD, TOK), BF16),
            dma((NZ,)), dma((NZ,)), dma((NG,)), dma((NG,)), dma((NY,)), dma((NY,)), dma((NY + 1,)),
        ],
        compiler_params=pltpu.CompilerParams(collective_id=1, has_side_effects=True),
        name="product",
    )(dqt, rb, normed_input, ag)

    dkv = pl.pallas_call(
        collect_kernel,
        grid=(NZ,),
        out_shape=shape((NZ, TOK, 128), BF16),
        in_specs=[
            smem,
            pl.BlockSpec((1, TOK, 128), lambda i: (i, 0, 0)),
            pl.BlockSpec((NG, SLOTS, KB, 128), lambda i: (0, 0, 0, 0)),
        ],
        out_specs=pl.BlockSpec((1, TOK, 128), lambda i: (i, 0, 0)),
        scratch_shapes=[pltpu.VMEM((TOK, 128), F32)],
        compiler_params=pltpu.CompilerParams(dimension_semantics=("arbitrary",)),
        name="collect",
    )(want, dkvo, rbr)

    dkvr, grad_weight = pl.pallas_call(
        return_kernel,
        out_shape=(shape((NZ, TOK, 128), BF16), shape((HD, TOK), F32)),
        in_specs=[vmem, vmem],
        out_specs=(hbm, vmem),
        scratch_shapes=[pltpu.VMEM((NZ, HD, TOK), BF16)] * 6
        + [dma((NZ,))] * 10
        + [dma((1,))],
        compiler_params=pltpu.CompilerParams(collective_id=2, has_side_effects=True),
        name="return",
    )(dkv, s1)

    width = NZ * HD
    grad_queries, grad_keys, grad_values = pl.pallas_call(
        unpack_kernel,
        grid=(NZ // 2,),
        out_shape=(shape((TOK, width), F32),) * 3,
        in_specs=[
            pl.BlockSpec((2, HD, TOK), lambda i: (i, 0, 0)),
            pl.BlockSpec((2, TOK, 128), lambda i: (i, 0, 0)),
        ],
        out_specs=(pl.BlockSpec((TOK, 128), lambda i: (0, i)),) * 3,
        compiler_params=pltpu.CompilerParams(dimension_semantics=("arbitrary",)),
        name="unpack",
    )(qbt, dkvr)
    return (grad_queries, grad_keys, grad_values, grad_weight)


def solution(mesh):
    return jax.shard_map(
        per_device,
        mesh=mesh,
        in_specs=(
            P("kv", "tp"),
            P("kv", "tp"),
            P("kv", "tp"),
            P("kv", "tp"),
            P("tp", "kv"),
            P("kv", "tp"),
            P("kv", None),
        ),
        out_specs=(P("kv", "tp"), P("kv", "tp"), P("kv", "tp"), P("kv", "tp")),
        check_vma=False,
    )
```

time: 444 us -> 183 us (0.41); the launches traced: 435 us -> 181 us
  waiting for transfers between devices: 221 us -> 0 us
  Pallas kernels: 0 us -> 178 us
  matrix products: 86.3 us -> 0 us
  local copies, waits for them, and re-layouts: 57.1 us -> 2.82 us
  other arithmetic: 20.2 us -> 0 us
  blocking collectives: 18.7 us -> 0 us
  starting transfers between devices: 17 us -> 0 us
  between operations: 14.3 us -> 0.66 us
    all_to_all x2 -> x0, waiting for transfers between devices: 194 us -> none  [in_one_piece(): lax.all_to_all(both, axis, split_axis=split_dim, concat_axis=concat_dim,...]
    pallas_call x0 -> x6, Pallas kernels: none -> 178 us  [the longest x1 71 us: per_device(): pl.pallas_call(gather_kernel, out_shape=(shape((NZ, BPD, KB, 128), BF16),...]
    dot_general x83 -> x0, matrix products: 86.3 us -> none  [the longest x81 85.5 us: contract(): lax.dot_general(former, latter, (((former_dim,), (latter_dim,)), ((), ())...]
    unnamed x3 -> x0, waiting for transfers between devices: 27.4 us -> none
    unnamed x28 -> x1, local copies, waits for them, and re-layouts: 21.5 us -> 1.57 us
    all_to_all x1 -> x0, blocking collectives: 18.7 us -> none  [per_device(): lax.all_to_all(wanted.reshape(kv_size, capacity), 'kv', split_axis=0, con...]
    all_to_all x2 -> x0, starting transfers between devices: 16.8 us -> none  [in_one_piece(): lax.all_to_all(both, axis, split_axis=split_dim, concat_axis=concat_dim,...]
    gather x4 -> x0, local copies, waits for them, and re-layouts: 8.14 us -> none  [the longest x1 2.98 us: per_device(): values_sel = got_values[picked].reshape(MOST * KB, width_here)]
  transfers between devices with their start and end apart: 4 -> 0, of which waited for: 3 -> 0; matrix products, arithmetic and copies ran while one was open for 31% -> 0% of each run, Pallas kernels for 0% -> 0%
where the time goes in v1:
time: 183 us; the launch traced here: 181 us
  Pallas kernels  178 us (97%)
  local copies, waits for them, and re-layouts  2.82 us (2%)
    pallas_call x1, Pallas kernels, per_device(): pl.pallas_call(gather_kernel, out_shape=(shape((NZ, BPD, KB, 128), BF16),...  71 us
    pallas_call x1, Pallas kernels, per_device(): pl.pallas_call(return_kernel, out_shape=(shape((NZ, TOK, 128), BF16), sha...  43.6 us
    pallas_call x1, Pallas kernels, per_device(): pl.pallas_call(product_kernel, out_shape=(shape((NZ, HD, TOK), BF16), sha...  33.6 us
    pallas_call x1, Pallas kernels, per_device(): pl.pallas_call(attention_kernel, grid=(NZ,), out_shape=(shape((NZ, HD, TO...  17.2 us
    pallas_call x1, Pallas kernels, per_device(): pl.pallas_call(collect_kernel, grid=(NZ,), out_shape=shape((NZ, TOK, 128)...  8.21 us
    pallas_call x1, Pallas kernels, per_device(): pl.pallas_call(unpack_kernel, grid=(NZ // 2,), out_shape=(shape((TOK, wid...  4.04 us

profile of v1, /device:TPU:73, one launch (start us, length us, event | category | flops | bytes accessed | tf_op | source)
XLA Modules:
  0.0 181.1 jit_solution(12338936584186725902)
XLA Ops:
  0.6 1.3 pad.4.list_ref
  1.9 71.0 %gather.1 = (bf16[8,16,32,128]{3,2,1,0:T(8,128)(2,1)}, bf16[8,16,32,128]{3,2,1,0:T(8,128)(2,1)}, f32[8,1,512]{2,1,0:T(1,128)}, bf16[8,36,32,128]{3,2,1,0:T(8,128...) custom-call(bf16[512,512]{1,0:T(8,128)(2,1)} %q_ref.1, bf16[512,512]{1,0:T(8,128)(2,1)} %k_ref.1, ...), custom_call_target="tpu_custom_call" | custom-call | tf_op jit(solution)/shard_map/gather/pallas_call | solution.py:489
  72.8 17.2 %attention.1 = (bf16[8,64,512]{2,1,0:T(8,128)(2,1)}, f32[8,512,128]{2,1,0:T(8,128)}, bf16[8,36,32,128]{3,2,1,0:T(8,128)(2,1)}) custom-call(s32[64,128]{1,0:T(8,128)} %get-tuple-element.22.t_ref, bf16[8,16,32,128]{3,2,1,0:T(8,128)(2,1)} %get-tuple-element.23.qo_ref, bf16[8,16,32,128]{3,2,1,0:T(8,128)(2,1)} %get-tuple-element.24.kv_ref, ...), custom_call_target="tpu_custom_call" | custom-call | tf_op jit(solution)/shard_map/attention/pallas_call | solution.py:516
  90.0 33.6 %product.1 = (bf16[8,64,512]{2,1,0:T(8,128)(2,1)}, bf16[8,36,32,128]{3,2,1,0:T(8,128)(2,1)}, bf16[32,64,512]{2,1,0:T(8,128)(2,1)}) custom-call(bf16[8,64,512]{2,1,0:T(8,128)(2,1)} %get-tuple-element.27.dq_ref, bf16[8,36,32,128]{3,2,1,0:T(8,128)(2,1)} %get-tuple-element.28.rb_ref, bf16[512,1024]{1,0:T(8,128)(2,1)} %a_ref.3, ...), custom_call_target="tpu_custom_call" | custom-call | tf_op jit(solution)/shard_map/product/pallas_call | solution.py:549
  123.6 8.2 %collect.1.dkv_ref = bf16[8,512,128]{2,1,0:T(8,128)(2,1)} custom-call(s32[64,128]{1,0:T(8,128)} %get-tuple-element.31.w_ref, f32[8,512,128]{2,1,0:T(8,128)} %get-tuple-element.32.own_ref, bf16[8,36,32,128]{3,2,1,0:T(8,128)(2,1)} %get-tuple-element.33.rbr_ref), custom_call_target="tpu_custom_call" | custom-call | tf_op jit(solution)/shard_map/collect/pallas_call | solution.py:570
  131.8 43.6 %return.1 = (bf16[8,512,128]{2,1,0:T(8,128)(2,1)}, f32[64,512]{1,0:T(8,128)}) custom-call(bf16[8,512,128]{2,1,0:T(8,128)(2,1)} %collect.1.dkv_ref, bf16[32,64,512]{2,1,0:T(8,128)(2,1)} %get-tuple-element.34.s1_ref), custom_call_target="tpu_custom_call" | custom-call | tf_op jit(solution)/shard_map/return/pallas_call | solution.py:585
  175.5 4.0 %unpack.1 = (f32[512,512]{1,0:T(8,128)}, f32[512,512]{1,0:T(8,128)}, f32[512,512]{1,0:T(8,128)}) custom-call(bf16[8,64,512]{2,1,0:T(8,128)(2,1)} %get-tuple-element.30.qbt_ref, bf16[8,512,128]{2,1,0:T(8,128)(2,1)} %get-tuple-element.35.dkv_ref), custom_call_target="tpu_custom_call" | custom-call | tf_op jit(solution)/shard_map/unpack/pallas_call | solution.py:598
  179.5 1.6 copy.12
